TPU v7x, 32 devices: a whole 2x2x4 slice. The times are simulated.
32 devices in a mesh: ep: 8 (over z, y), tp: 4 (over x, core).
Axes of the slice: x: 2, y: 2, z: 4, core: 2. Of those that a mesh axis runs over, the one named last changes fastest.
Arguments:
- queries: bfloat16 [4096, 2048], P('ep', 'tp'), may hold values from -6 to 6
- key_rows: bfloat16 [4096, 2048], P('ep', 'tp'), may hold values from -6 to 6
- value_rows: bfloat16 [4096, 4096], P('ep', 'tp'), may hold values from -6 to 6
- gate_rows: bfloat16 [4096, 4096], P('ep', 'tp'), may hold values from -6 to 6
- log_decay: float32 [16, 4096], P('tp', 'ep'), may hold values from -1 to 0
- head_gain: float32 [4096], P('tp'), may hold values from 0.1 to 1.9
- out_weight: bfloat16 [4096, 4096], P('tp'), may hold values from -0.09375 to 0.09375
- expert_input: bfloat16 [4096, 4096], P('ep'), may hold values from -6 to 6
- input_gain: float32 [4096], replicated, may hold values from 0.1 to 1.9
- route_ids: int32 [4096, 2], P('ep'), may hold values from 0 to 7, as said below
- route_weight: float32 [4096, 2], P('ep'), may hold values from 0.1 to 0.9
- expert_gate: bfloat16 [8, 4096, 1024], P('ep', None, 'tp'), may hold values from -0.09375 to 0.09375
- expert_up: bfloat16 [8, 4096, 1024], P('ep', None, 'tp'), may hold values from -0.09375 to 0.09375
- expert_down: bfloat16 [8, 1024, 4096], P('ep', 'tp'), may hold values from -0.1875 to 0.1875
Outputs:
- mixer_out: bfloat16 [4096, 4096], P(('ep', 'tp'))
- expert_out: bfloat16 [4096, 4096], P('ep', 'tp')
Inputs may be any that keep to these rules, and one draw needn't show every extreme that they name: `route_ids`: each row names two different experts of one group of 8 consecutive experts. On the rows of one device each group is named by exactly 512 rows, experts 2 i and 2 i + 1 together are named exactly 4 * 192 / 3 times, and no expert is named by more than 192 rows; one expert is named by exactly 192 rows of every device.
All inputs are finite; a program needn't handle non-finite values.
Results may differ from a plain program's by a relative error of at most 0.019.
Values may be sent and summed in bfloat16 or wider, within the bound.
No kernel may reach another device: no remote copies, remote signals or barrier semaphores. Data moves between devices by JAX's collectives and lax.ppermute only.
A program may use at most 192 MiB of HBM per device.

v0:
```python
import jax
import jax.numpy as jnp
from jax import lax
from jax.sharding import PartitionSpec as P

BLOCK = 512


epsilon = 1e-06
theta_base = 10000.0
largest_entry = lax.Precision.HIGHEST


def prefix(value, axis, combine, identity):
    length, index = (lax.axis_size(axis), lax.axis_index(axis))
    everything = jax.tree.map(
        lambda part, kind: lax.all_gather(part.astype(kind), axis),
        value,
        (jnp.bfloat16, jnp.bfloat16),
    )
    start = jax.tree.map(
        lambda part, zero: jnp.broadcast_to(jnp.asarray(zero, part.dtype), part.shape),
        value,
        identity,
    )

    def hop(k, before):
        reached = k < index
        new = combine(
            before, jax.tree.map(lambda part, own: part[k].astype(own.dtype), everything, value)
        )
        return jax.tree.map(lambda a, b: jnp.where(reached, a, b), new, before)

    return lax.fori_loop(0, length, hop, start)


def rotate(values, positions):
    half_dim = values.shape[-1] // 2
    frequency = theta_base ** (-jnp.arange(half_dim, dtype=jnp.float32) / half_dim)
    angles = positions.astype(jnp.float32)[:, None, None] * frequency
    cosine = jnp.cos(angles)
    sine_wave = jnp.sin(angles)
    first_half = values[..., :half_dim]
    second = values[..., half_dim:]
    return jnp.concatenate(
        [first_half * cosine - second * sine_wave, second * cosine + first_half * sine_wave],
        axis=-1,
    )


def round_back(values):
    return lax.optimization_barrier(values.astype(jnp.bfloat16)).astype(jnp.float32)


def to_blocks(array, blocks):
    return array.reshape(blocks, array.shape[0] // blocks, array.shape[1], array.shape[2])


def combine_states(earlier, later):
    return (later[1][:, None, None] * earlier[0] + later[0], earlier[1] * later[1])


def retention_rows(queries, key_rows, value_rows, gate_rows, log_decay, head_gain):
    length = queries.shape[0]
    head_count = log_decay.shape[0]
    key_width = queries.shape[1] // head_count
    value_width = value_rows.shape[1] // head_count
    blocks = length // BLOCK
    positions = lax.axis_index("ep") * length + jnp.arange(length, dtype=jnp.int32)
    query_rot = to_blocks(
        rotate(queries.astype(jnp.float32).reshape(length, head_count, key_width), positions),
        blocks,
    )
    key_rot = to_blocks(
        rotate(key_rows.astype(jnp.float32).reshape(length, head_count, key_width), positions)
        * key_width ** (-0.5),
        blocks,
    )
    value_all = to_blocks(
        value_rows.astype(jnp.float32).reshape(length, head_count, value_width), blocks
    )
    running = jnp.cumsum(log_decay.reshape(head_count, blocks, BLOCK), axis=2)
    ending = running[:, :, -1]
    kept = jnp.exp(ending[:, :, None] - running)
    block_states = jnp.einsum(
        "nlhd,hnl,nlhe->nhde", key_rot, kept, value_all, precision=largest_entry
    )
    block_decay = jnp.exp(ending).T

    def advance(carried, inputs):
        decay_now, state_now = inputs
        return (decay_now[:, None, None] * carried + state_now, carried)

    zeros_state = jnp.zeros((head_count, key_width, value_width), jnp.float32)
    device_state, local_starts = lax.scan(advance, zeros_state, (block_decay, block_states))
    device_decay = jnp.exp(jnp.sum(ending, axis=1))
    incoming, passed_decay = prefix(
        (device_state, device_decay),
        "ep",
        combine_states,
        (zeros_state, jnp.ones((head_count,), jnp.float32)),
    )
    causal = jnp.arange(BLOCK)[:, None] >= jnp.arange(BLOCK)[None, :]
    spread = running[:, :, :, None] - running[:, :, None, :]
    weight_table = jnp.exp(jnp.where(causal, spread, -jnp.inf))
    score_matrix = (
        jnp.einsum("nlhd,nmhd->hnlm", query_rot, key_rot, precision=largest_entry) * weight_table
    )
    inside = jnp.einsum("hnlm,nmhe->nlhe", score_matrix, value_all, precision=largest_entry)
    before = jnp.exp(jnp.cumsum(ending, axis=1) - ending)
    starts = local_starts + before.T[:, :, None, None] * incoming[None]
    outside = jnp.einsum(
        "nlhd,hnl,nhde->nlhe", query_rot, jnp.exp(running), starts, precision=largest_entry
    )
    mixed = (inside + outside).reshape(length, head_count, value_width)
    centered = mixed - jnp.mean(mixed, axis=-1, keepdims=True)
    normed = (
        centered
        * lax.rsqrt(jnp.mean(centered * centered, axis=-1, keepdims=True) + epsilon)
        * head_gain.reshape(head_count, value_width)
    )
    return (
        jax.nn.silu(gate_rows.astype(jnp.float32))
        * normed.reshape(length, head_count * value_width)
    ).astype(jnp.bfloat16)


def body(
    queries,
    key_rows,
    value_rows,
    gate_rows,
    log_decay,
    head_gain,
    out_weight,
    expert_input,
    input_gain,
    route_ids,
    route_weight,
    expert_gate,
    expert_up,
    expert_down,
):
    hidden = retention_rows(queries, key_rows, value_rows, gate_rows, log_decay, head_gain)
    tp_count = lax.axis_size("tp")
    model_width = out_weight.shape[1]
    mixer_out = lax.psum_scatter(
        jnp.dot(hidden, out_weight, preferred_element_type=jnp.float32).astype(jnp.bfloat16),
        "tp",
        scatter_dimension=0,
        tiled=True,
    )
    token_count = expert_input.shape[0]
    local_experts = expert_gate.shape[0]
    ep_count = lax.axis_size("ep")
    expert_count = ep_count * local_experts
    capacity = 3 * token_count // expert_count
    quarter = model_width // tp_count
    widened = expert_input.astype(jnp.float32)
    normed = (
        widened
        * lax.rsqrt(jnp.mean(widened * widened, axis=-1, keepdims=True) + epsilon)
        * input_gain
    ).astype(jnp.bfloat16)
    flat_ids = route_ids.reshape(-1)
    matches = (flat_ids[:, None] == jnp.arange(expert_count, dtype=jnp.int32)[None, :]).astype(
        jnp.int32
    )
    slot_rank = jnp.sum((jnp.cumsum(matches, axis=0) - matches) * matches, axis=1)
    target = flat_ids * capacity + slot_rank
    owners = jnp.arange(2 * token_count, dtype=jnp.int32) // 2
    slot_table = jnp.full((expert_count * capacity,), token_count, jnp.int32).at[target].set(owners)
    padded = jnp.concatenate([normed, jnp.zeros((1, model_width), jnp.bfloat16)], axis=0)
    share = capacity // tp_count
    own_slots = lax.dynamic_slice_in_dim(
        slot_table.reshape(expert_count, capacity), lax.axis_index("tp") * share, share, 1
    )
    outgoing = padded[own_slots]
    arrived = lax.all_to_all(outgoing, "ep", split_axis=0, concat_axis=0, tiled=True).reshape(
        ep_count, local_experts, share, model_width
    )
    gate_whole, up_whole, down_whole = (
        lax.all_gather(expert_gate, "tp", axis=2, tiled=True),
        lax.all_gather(expert_up, "tp", axis=2, tiled=True),
        lax.all_gather(expert_down, "tp", axis=1, tiled=True),
    )
    gate_val = jnp.einsum("sxcd,xdf->sxcf", arrived, gate_whole, preferred_element_type=jnp.float32)
    up_val = jnp.einsum("sxcd,xdf->sxcf", arrived, up_whole, preferred_element_type=jnp.float32)
    inner_rows = (jax.nn.silu(gate_val) * up_val).astype(jnp.bfloat16)
    unit_group = expert_down.shape[1]
    group_parts = jnp.einsum(
        "sxcgf,xgfd->gsxcd",
        inner_rows.reshape(ep_count, local_experts, share, tp_count, unit_group),
        down_whole.reshape(local_experts, tp_count, unit_group, model_width),
        preferred_element_type=jnp.float32,
    )
    finished = jnp.sum(round_back(group_parts), axis=0).astype(jnp.bfloat16)
    came_back = lax.all_to_all(finished, "ep", split_axis=0, concat_axis=0, tiled=True)
    returned = lax.all_to_all(came_back, "tp", split_axis=3, concat_axis=2, tiled=True).reshape(
        expert_count * capacity, quarter
    )
    picked = returned[target].reshape(token_count, 2, quarter).astype(jnp.float32)
    expert_out = jnp.sum(picked * route_weight[:, :, None], axis=1).astype(jnp.bfloat16)
    return (mixer_out, expert_out)


def solution(mesh):
    placed = (
        P("ep", "tp"),
        P("ep", "tp"),
        P("ep", "tp"),
        P("ep", "tp"),
        P("tp", "ep"),
        P("tp"),
        P("tp", None),
        P("ep", None),
        P(),
        P("ep", None),
        P("ep", None),
        P("ep", None, "tp"),
        P("ep", None, "tp"),
        P("ep", "tp", None),
    )
    return jax.shard_map(
        body,
        mesh=mesh,
        in_specs=placed,
        out_specs=(P(("ep", "tp"), None), P("ep", "tp")),
        check_vma=False,
    )
```

profile of v0, /device:TPU:0, one launch (start us, length us, event | category | flops | bytes accessed | tf_op | source)
XLA Modules:
  0.0 503.5 jit_solution(17845343262958947994)
XLA Ops:
  7.9 1.2 reduce-window.14
  9.5 1.3 copy.69
  10.9 1.3 copy.100
  12.3 1.4 copy.101
  14.0 1.3 copy.102
  15.3 1.3 copy.103
  18.2 4.1 multiply_subtract_fusion
  22.3 3.2 fusion.36
  28.2 2.3 reduce-window.16
  31.4 4.8 scatter_custom_fusion
  38.0 3.1 fusion.1
  41.1 1.7 fusion.3
  42.8 2.5 concatenate.14
  45.3 11.0 %gather_fusion = bf16[384,4096]{1,0:T(8,128)(2,1)} fusion(bf16[513,4096]{1,0:T(8,128)(2,1)} %concatenate.14, s32[1024]{0:T(1024)S(1)} %pad_clamp_fusion), kind=kCustom, calls=%fused_computation | custom fusion | bytes 6292992 | tf_op jit(solution)/shard_map/gather | solution.py:178
  56.5 7.2 %all-to-all-start = ((bf16[8,48,4096]{2,1,0:T(8,128)(2,1)}), bf16[8,48,4096]{2,1,0:T(8,128)(2,1)}, u32[]{:S(2)}, u32[]{:S(2)}) async-start(bf16[8,48,4096]{2,1,0:T(8,128)(2,1)} %bitcast.27), calls=%async_computation.1 | async-start | bytes 6291456 | tf_op jit(solution)/shard_map/all_to_all | solution.py:179
  63.8 74.5 %all-reduce.1 = bf16[32]{0:T(256)(128)(2,1)S(1)} all-reduce(bf16[32]{0:T(256)(128)(2,1)S(1)} %dynamic-update-slice), channel_id=2, replica_groups=mesh['ep'=8,'tp'=4] {'ep'}, use_global_device_ids=true, to_apply=%add.1 | all-reduce | flops 32 | bytes 128
  138.4 5.4 %fusion.50 = f32[4,512,512]{2,1,0:T(8,128)S(1)} fusion(f32[512,4,64]{2,0,1:T(8,128)} %get-tuple-element.148, f32[512,4,64]{2,0,1:T(8,128)} %get-tuple-element.149, f32[512,4,64]{2,0,1:T(8,128)S(1)} %get-tuple-element.145, f32[512,4,64]{2,0,1:T(8,128)S(1)} %get-tuple-element.144), kind=kOutput, calls=%fused_computation.70 | convolution fusion | flops 1611399168 | bytes 6291456 | tf_op jit(solution)/shard_map/nlhd,nmhd->hnlm/dot_general | solution.py:107
  143.9 4.6 fusion.8
  148.5 9.1 %while.9 = (s32[]{:T(128)}, f32[4,128,256]{2,1,0:T(8,128)S(1)}, s32[]{:T(128)}, bf16[8,4]{1,0:T(8,128)(2,1)S(1)}, bf16[8,4,128,256]{3,2,1,0:T(8,128)(2,1)}, /*index=5*/s32[]{:T(128)}, s32[]{:T(128)}) while((s32[]{:T(128)}, f32[4,128,256]{2,1,0:T(8,128)S(1)}, s32[]{:T(128)}, bf16[8,4]{1,0:T(8,128)(2,1)S(1)}, ...), condition=%wide.region_3.4_spmd.clone, body=%wide.region_2.3_spmd.clone.sunk | while | flops 655368 | bytes 1310865 | solution.py:34
  148.5 1.1 fusion.77
  149.6 1.1 fusion.77
  150.8 1.1 fusion.77
  151.9 1.1 fusion.77
  153.0 1.1 fusion.77
  156.4 1.1 fusion.77
  157.5 4.9 fusion.71
  163.5 1.8 copy.106
  165.3 1.6 sub.70
  166.9 2.9 copy.84
  169.7 2.0 copy.83
  171.8 12.7 %convolution_convert_fusion = bf16[512,4096]{1,0:T(8,128)(2,1)} fusion(bf16[1024,4096]{1,0:T(8,128)(2,1)} %param.22, f32[512,1024]{1,0:T(8,128)} %bitcast.162, f32[512,1024]{1,0:T(8,128)} %copy.83, f32[512,1024]{1,0:T(8,128)} %copy.84, bf16[512,1024]{1,0:T(8,128)(2,1)} %param.19, f32[1024]{0:T(1024)S(1)} %copy-done.7), kind=kOutput, calls=%fused_computation.16 | convolution fusion | flops 4302307328 | bytes 19927040 | tf_op jit(solution)/shard_map/dot_general | solution.py:148
  184.5 7.2 %fusion.6 = f32[8,48,1024]{2,1,0:T(8,128)S(1)} fusion(bf16[8,48,4096]{2,1,0:T(8,128)(2,1)} %all-to-all-done, bf16[1,4096,1024]{2,1,0:T(8,128)(2,1)} %all-gather.7.cloned.1.call-done), kind=kOutput, calls=%fused_computation.14 | convolution fusion | flops 3221225472 | bytes 13107200 | tf_op jit(solution)/shard_map/sxcd,xdf->sxcf/dot_general | solution.py:187
  191.7 41.9 %all-gather.9.cloned.1.call-done = bf16[1,4096,1024]{2,1,0:T(8,128)(2,1)} async-done(((bf16[1,4096,256]{2,1,0:T(8,128)(2,1)}), bf16[1,4096,1024]{2,1,0:T(8,128)(2,1)}) %all-gather.9.cloned.1.call-update) | async-done | bytes 8388624 | tf_op jit(solution)/shard_map/all_gather | solution.py:184
  233.6 7.9 %fusion.27 = bf16[8,1,48,1024]{3,2,0,1:T(8,128)(2,1)S(1)} fusion(f32[8,48,1024]{2,1,0:T(8,128)S(1)} %fusion.6, bf16[8,48,4096]{2,1,0:T(8,128)(2,1)} %all-to-all-done, bf16[1,4096,1024]{2,1,0:T(8,128)(2,1)} %all-gather.9.cloned.1.call-done), kind=kOutput, calls=%fused_computation.42 | convolution fusion | flops 3223584768 | bytes 13893632 | tf_op jit(solution)/shard_map/sxcd,xdf->sxcf/dot_general | solution.py:188
  242.1 51.3 %all-gather.11.cloned.1.call-done = bf16[1,1024,4096]{2,1,0:T(8,128)(2,1)} async-done(((bf16[1,256,4096]{2,1,0:T(8,128)(2,1)}), bf16[1,1024,4096]{2,1,0:T(8,128)(2,1)}) %all-gather.11.cloned.1.call-update) | async-done | bytes 8388624 | tf_op jit(solution)/shard_map/all_gather | solution.py:185
  293.3 10.3 %convert_bitcast_fusion = bf16[4,8,1,48,4096]{4,3,1,0,2:T(8,128)(2,1)} fusion(bf16[4,256,4096,1]{2,1,3,0:T(8,128)(2,1)} %bitcast.159, bf16[8,48,4,256]{3,2,1,0:T(4,128)(2,1)S(1)} %reshape.414), kind=kOutput, calls=%fused_computation.6 | convolution fusion | flops 3227516928 | bytes 21757952 | tf_op jit(solution)/shard_map/sxcgf,xgfd->gsxcd/dot_general | solution.py:191
  303.6 8.6 %reduce_sum.70 = bf16[8,48,4096]{2,1,0:T(8,128)(2,1)S(1)} reduce(bf16[4,8,1,48,4096]{4,3,1,0,2:T(8,128)(2,1)} %convert_bitcast_fusion, bf16[]{:T(256)} %constant.105.clone.1), dimensions={0,2}, to_apply=%region_12.13 | reduce | flops 4718592 | bytes 15728642 | tf_op jit(solution)/shard_map/reduce_sum | solution.py:197
  312.2 76.6 %all_to_all.25 = bf16[8,1,48,4096]{3,2,1,0:T(8,128)(2,1)} all-to-all(bf16[8,1,48,4096]{3,2,1,0:T(8,128)(2,1)S(1)} %bitcast.155), channel_id=1, replica_groups=mesh['ep'=8,'tp'=4] {'ep'}, dimensions={0} | all-to-all | bytes 6291456 | tf_op jit(solution)/shard_map/all_to_all | solution.py:198
  388.8 9.7 %copy.90 = bf16[8,1,48,4096]{2,0,1,3:T(8,128)(2,1)} copy(bf16[8,1,48,4096]{3,2,1,0:T(8,128)(2,1)} %all_to_all.25) | data formatting | bytes 6291456 | tf_op jit(solution)/shard_map/all_to_all | solution.py:198
  398.5 14.8 %reshape.467 = bf16[4,2,196608]{2,1,0:T(2,128)(2,1)} reshape(bf16[4096,1,8,48]{3,2,1,0:T(8,128)(2,1)} %bitcast.152) | data formatting | bytes 6291456
  413.3 4.0 all-to-all-start.2
  417.5 36.7 %all-to-all-done.2 = bf16[4,2,196608]{2,1,0:T(2,128)(2,1)S(1)} async-done(((bf16[4,2,196608]{2,1,0:T(2,128)(2,1)}), bf16[4,2,196608]{2,1,0:T(2,128)(2,1)S(1)}, u32[]{:S(2)}, u32[]{:S(2)}) %all-to-all-start.2) | async-done | bytes 3145760 | tf_op jit(solution)/shard_map/all_to_all | solution.py:199
  454.2 9.9 %reshape.468 = bf16[4096,1,8,48]{3,2,1,0:T(8,128)(2,1)} reshape(bf16[4,2,196608]{2,1,0:T(2,128)(2,1)S(1)} %all-to-all-done.2) | data formatting | bytes 6291456
  464.1 10.2 %copy.99 = bf16[8,1,48,4,1024]{4,3,2,0,1:T(4,128)(2,1)} copy(bf16[8,1,48,4,1024]{2,0,4,3,1:T(8,128)(2,1)} %bitcast.153) | data formatting | bytes 6291456 | tf_op jit(solution)/shard_map/all_to_all | solution.py:199
  474.3 3.0 copy.92
  477.3 5.4 %gather_fusion.1 = bf16[1024,1024]{1,0:T(8,128)(2,1)} fusion(bf16[1536,1024]{1,0:T(8,128)(2,1)S(1)} %bitcast.151, s32[1024]{0:T(1024)S(1)} %broadcast_clamp_fusion), kind=kCustom, calls=%fused_computation.1 | custom fusion | bytes 4198400 | tf_op jit(solution)/shard_map/gather | solution.py:202
  482.7 5.4 %reshape.423 = f32[512,2,1024]{2,1,0:T(2,128)} reshape(bf16[1024,1024]{1,0:T(8,128)(2,1)} %gather_fusion.1) | data formatting | bytes 6291456 | tf_op jit(solution)/shard_map/convert_element_type | solution.py:202
  488.2 8.6 %multiply_reduce_fusion = bf16[512,1024]{1,0:T(8,128)(2,1)} fusion(f32[512,2,1024]{2,1,0:T(2,128)} %reshape.423, f32[512,2]{1,0:T(8,128)S(1)} %copy.93), kind=kLoop, calls=%fused_computation.17 | loop fusion | flops 1572864 | bytes 5246976 | tf_op jit(solution)/shard_map/reduce_sum | solution.py:203
  (92 shorter events, 11.8 us)
Async XLA Ops:
  7.2 141.3 %all-gather.13.cloned.1.call-start = ((), (), s32[]{:S(2)}) async-start(), calls=%async_computation.8 | async-start | bytes 2359296 | tf_op jit(solution)/shard_map/all_gather | solution.py:17
  9.5 4.2 copy-start.3
  18.2 4.1 copy-start.1
  25.5 2.1 copy-start.5
  25.5 159.0 %all-gather.7.cloned.1.call-start = ((), (), s32[]{:S(2)}) async-start(), calls=%async_computation.5 | async-start | bytes 10485760 | tf_op jit(solution)/shard_map/all_gather | solution.py:183
  26.3 10.1 %copy-start.8 = (u32[32]{0:T(128)S(1)}, u32[32]{0:T(128)}, u32[]{:S(2)}) copy-start(u32[32]{0:T(128)} %constant.120) | copy-start | bytes 388
  26.3 207.3 %all-gather.9.cloned.1.call-start = ((), (), s32[]{:S(2)}) async-start(), calls=%async_computation.6 | async-start | bytes 10485760 | tf_op jit(solution)/shard_map/all_gather | solution.py:184
  27.0 266.3 %all-gather.11.cloned.1.call-start = ((), (), s32[]{:S(2)}) async-start(), calls=%async_computation.7 | async-start | bytes 10485760 | tf_op jit(solution)/shard_map/all_gather | solution.py:185
  27.6 13.5 %copy-start.4 = (f32[4096]{0:T(1024)S(1)}, f32[4096]{0:T(1024)}, u32[]{:S(2)}) copy-start(f32[4096]{0:T(1024)} %param.24) | copy-start | bytes 49156
  36.4 4.7 copy-start
  56.5 128.0 %all-to-all-start = ((bf16[8,48,4096]{2,1,0:T(8,128)(2,1)}), bf16[8,48,4096]{2,1,0:T(8,128)(2,1)}, u32[]{:S(2)}, u32[]{:S(2)}) async-start(bf16[8,48,4096]{2,1,0:T(8,128)(2,1)} %bitcast.27), calls=%async_computation.1 | async-start | bytes 6291456 | tf_op jit(solution)/shard_map/all_to_all | solution.py:179
  63.7 433.0 %reduce-scatter.2.cloned.1.call-start = ((), (), s32[]{:S(2)}) async-start(), calls=%async_computation.4 | async-start | bytes 5242880 | tf_op jit(solution)/shard_map/reduce_scatter | solution.py:147
  138.4 5.5 %copy-start.2 = (bf16[512,1024]{1,0:T(8,128)(2,1)S(1)}, bf16[512,1024]{1,0:T(8,128)(2,1)}, u32[]{:S(2)}) copy-start(bf16[512,1024]{1,0:T(8,128)(2,1)} %param.18) | copy-start | bytes 3145732
  169.7 2.0 copy-start.7
  413.3 4.0 copy-start.6
  413.3 40.9 %all-to-all-start.2 = ((bf16[4,2,196608]{2,1,0:T(2,128)(2,1)}), bf16[4,2,196608]{2,1,0:T(2,128)(2,1)S(1)}, u32[]{:S(2)}, u32[]{:S(2)}) async-start(bf16[4,2,196608]{2,1,0:T(2,128)(2,1)} %reshape.467), calls=%async_computation.3 | async-start | bytes 6291456 | tf_op jit(solution)/shard_map/all_to_all | solution.py:199
Sparse Core Ops, SparseCore 0:
  25.7 72.0 all-gather.12
  99.3 73.2 all-gather.6
  174.2 59.3 all-gather.8
  235.0 58.2 all-gather.10
  296.3 44.5 reduce-scatter.1
where the time goes:
time: 511 us; the launch traced here: 503 us
  blocking collectives  151 us (30%)
  waiting for transfers between devices  132 us (26%)
  local copies, waits for them, and re-layouts  97 us (19%)
  matrix products  56.1 us (11%)
  other arithmetic  40.3 us (8%)
  between operations  15.4 us (3%)
  starting transfers between devices  11.4 us (2%)
    all_to_all x1, blocking collectives, body(): lax.all_to_all(finished, 'ep', split_axis=0, concat_axis=0, tiled=True)  76.6 us
    unnamed x1, blocking collectives  74.5 us
    all_gather x1, waiting for transfers between devices, body(): lax.all_gather(expert_down, 'tp', axis=1, tiled=True)  51.3 us
    all_gather x1, waiting for transfers between devices, body(): lax.all_gather(expert_up, 'tp', axis=2, tiled=True)  41.9 us
    all_to_all x1, waiting for transfers between devices, body(): lax.all_to_all(came_back, 'tp', split_axis=3, concat_axis=2, tiled=True)  36.7 us
    unnamed x32, local copies, waits for them, and re-layouts  34.6 us
    all_to_all x2, local copies, waits for them, and re-layouts, body(): lax.all_to_all(came_back, 'tp', split_axis=3, concat_axis=2, tiled=True)  13.2 us
    dot_general x1, matrix products, body(): jnp.dot(hidden, out_weight, preferred_element_type=jnp.float32)  12.7 us
  transfers between devices with their start and end apart: 7, of which 3 were waited for; matrix products, arithmetic and copies ran while one was open for 35% of the time, Pallas kernels for 0%

commit v1 on v0

v1 whole, which is shorter than its diff:
```python
import functools

import jax
import jax.numpy as jnp
from jax import lax
from jax.experimental import pallas as pl
from jax.experimental.pallas import tpu as pltpu
from jax.sharding import PartitionSpec as P


epsilon = 1e-06
theta_base = 10000.0
f32, bf16 = jnp.float32, jnp.bfloat16


def swap(value, axis, mask):
    size = lax.axis_size(axis)
    return lax.ppermute(value, axis, [(i, i ^ mask) for i in range(size)])


def dot(a, b):
    return jnp.dot(a, b, preferred_element_type=f32)


def turn(v, cosine, sine):
    half = v.shape[-1] // 2
    other = jnp.concatenate([v[:, half:], v[:, :half]], axis=-1)
    return v * cosine + other * sine


def split(v):
    high = v.astype(bf16)
    return high, (v - high.astype(f32)).astype(bf16)


def contract(a, b, dims):
    return lax.dot_general(a, b, (dims, ((), ())), preferred_element_type=f32)


def message(state, decay):
    high = decay.astype(bf16).astype(f32)
    tail = jnp.concatenate([high, decay - high], axis=-2)
    return state.astype(bf16), tail.astype(bf16)


def inside_kernel(
    q_ref, k_ref, v_ref, cos_ref, sin_ref, log_ref, o_ref, qd_ref, s_ref, d_ref, m_ref, rows, cols
):
    length, width = q_ref.shape
    out = v_ref.shape[1]
    heads = log_ref.shape[0]
    head = pl.program_id(0)
    later = lax.broadcasted_iota(jnp.int32, (length, length), 0)
    earlier = lax.broadcasted_iota(jnp.int32, (length, length), 1)
    causal = later >= earlier

    @pl.when(head == 0)
    def _():
        log = log_ref[...]
        high = log.astype(bf16).astype(f32)
        middle = (log - high).astype(bf16).astype(f32)
        ones = jnp.where(causal, 1.0, 0.0).astype(bf16)
        pad = jnp.zeros((8 - heads, length), f32)
        row, col = 0.0, 0.0
        for piece in (high, middle, log - high - middle):
            piece = jnp.concatenate([piece, pad], axis=0).astype(bf16)
            row += contract(piece, ones, ((1,), (1,)))
            col += contract(ones, piece, ((1,), (1,)))
        rows[...] = row
        cols[...] = col

    cosine, sine = cos_ref[...], sin_ref[...]
    q = turn(q_ref[...].astype(f32), cosine, sine)
    k = turn(k_ref[...].astype(f32), cosine, sine) * width ** (-0.5)
    v = v_ref[...]
    row = rows[pl.ds(head, 1), :]
    which = lax.broadcasted_iota(jnp.int32, (length, 8), 1)
    col = jnp.sum(jnp.where(which == head, cols[...], 0.0), axis=1, keepdims=True)
    ending = row[:, length - 1 :]
    kept_high, kept_low = split(k * jnp.exp(ending - col))
    kept = contract(jnp.concatenate([kept_high, kept_low], axis=1), v, ((0,), (0,)))
    state = kept[:width] + kept[width:]
    decay = jnp.broadcast_to(jnp.exp(ending), (8, out))
    s_ref[0] = state
    d_ref[0] = decay
    m_ref[0, :width], m_ref[0, width:] = message(state, decay)
    q_high, q_low = split(q)
    k_high, k_low = split(k)
    q_both = jnp.concatenate([q_high, q_low], axis=1)
    k_twice = jnp.concatenate([k_high, k_high], axis=1)
    last = ((1,), (1,))
    scores = contract(q_both, k_twice, last) + contract(q_high, k_low, last)
    weight = jnp.exp(jnp.where(causal, col - row, -jnp.inf))
    o_ref[...] = dot((scores * weight).astype(bf16), v)
    qd_ref[...] = q * jnp.exp(col)


def combine_kernel(late_ref, got_ref, s_ref, d_ref, *refs):
    width = s_ref.shape[1]
    late = late_ref[0] > 0
    other = got_ref[:, :width].astype(f32)
    tail = got_ref[:, width:].astype(f32)
    other_decay = tail[:, :8] + tail[:, 8:]
    state, decay = s_ref[...], d_ref[...]
    if len(refs) in (3, 7):
        before, before_decay = refs[0][...], refs[1][...]
        outs = refs[2:]
        outs[0][...] = jnp.where(late, before_decay[:, :1] * other + before, before)
    else:
        before_decay = jnp.ones_like(decay)
        outs = refs
        outs[0][...] = jnp.where(late, other, 0.0)
    if len(outs) == 1:
        return
    outs[1][...] = jnp.where(late, before_decay * other_decay, before_decay)
    state = jnp.where(late, decay[:, :1] * other + state, other_decay[:, :1] * state + other)
    decay = decay * other_decay
    outs[2][...] = state
    outs[3][...] = decay
    outs[4][:, :width], outs[4][:, width:] = message(state, decay)


def outside_kernel(o_ref, qd_ref, s_ref, gate_ref, gain_ref, h_ref):
    q_high, q_low = split(qd_ref[...])
    state = s_ref[0].astype(bf16)
    o = o_ref[...] + (dot(q_high, state) + dot(q_low, state))
    centered = o - jnp.mean(o, axis=-1, keepdims=True)
    scale = lax.rsqrt(jnp.mean(centered * centered, axis=-1, keepdims=True) + epsilon)
    gate = gate_ref[...].astype(f32)
    h_ref[...] = (gate / (1.0 + jnp.exp(-gate)) * (centered * scale * gain_ref[...])).astype(bf16)


def shapes(*arrays):
    return [jax.ShapeDtypeStruct(a.shape, a.dtype) for a in arrays]


def combine(final, late, got, state, decay, *before):
    results = [state, decay, state, decay, got]
    results = results[:1] if final else results
    return pl.pallas_call(
        combine_kernel,
        in_specs=[pl.BlockSpec(memory_space=pltpu.SMEM)] + [pl.BlockSpec()] * (3 + len(before)),
        out_shape=shapes(*results),
        name="combine",
    )(late, got, state, decay, *before)


def retention_inside(queries, key_rows, value_rows, log_decay):
    length = queries.shape[0]
    heads = log_decay.shape[0]
    width = queries.shape[1] // heads
    out = value_rows.shape[1] // heads
    half = width // 2
    positions = lax.axis_index("ep") * length + jnp.arange(length, dtype=jnp.int32)
    frequency = theta_base ** (-jnp.arange(half, dtype=f32) / half)
    angles = positions.astype(f32)[:, None] * frequency
    cosine, sine = jnp.cos(angles), jnp.sin(angles)
    cosine = jnp.concatenate([cosine, cosine], axis=-1)
    sine = jnp.concatenate([-sine, sine], axis=-1)
    whole = lambda *shape: pl.BlockSpec(shape, lambda h: (0,) * len(shape))
    cols = lambda n: pl.BlockSpec((length, n), lambda h: (0, h))
    first = lambda *shape: pl.BlockSpec((1,) + shape, lambda h: (h, 0, 0))
    return pl.pallas_call(
        inside_kernel,
        grid=(heads,),
        in_specs=[
            cols(width),
            cols(width),
            cols(out),
            whole(length, width),
            whole(length, width),
            whole(heads, length),
        ],
        out_specs=[cols(out), cols(width), first(width, out), first(8, out), first(width + 16, out)],
        out_shape=[
            jax.ShapeDtypeStruct((length, heads * out), f32),
            jax.ShapeDtypeStruct((length, heads * width), f32),
            jax.ShapeDtypeStruct((heads, width, out), f32),
            jax.ShapeDtypeStruct((heads, 8, out), f32),
            jax.ShapeDtypeStruct((heads, width + 16, out), bf16),
        ],
        scratch_shapes=[pltpu.VMEM((8, length), f32), pltpu.VMEM((length, 8), f32)],
        cost_estimate=pl.CostEstimate(
            flops=8 * heads * length * length * out, bytes_accessed=2**23, transcendentals=2**21
        ),
        name="inside",
    )(queries, key_rows, value_rows, cosine, sine, log_decay)


def retention_outside(inside, turned, incoming, gate_rows, head_gain):
    length = inside.shape[0]
    heads, width, out = incoming.shape
    cols = lambda n: pl.BlockSpec((length, n), lambda h: (0, h))
    first = lambda *shape: pl.BlockSpec((1,) + shape, lambda h: (h, 0, 0))
    return pl.pallas_call(
        outside_kernel,
        grid=(heads,),
        in_specs=[
            cols(out),
            cols(width),
            first(width, out),
            cols(out),
            pl.BlockSpec((1, out), lambda h: (0, h)),
        ],
        out_specs=cols(out),
        out_shape=jax.ShapeDtypeStruct((length, heads * out), bf16),
        cost_estimate=pl.CostEstimate(
            flops=8 * length * heads * out * width, bytes_accessed=2**22, transcendentals=2**19
        ),
        name="outside",
    )(inside, turned, incoming, gate_rows, head_gain[None, :])


def mixer_kernel(core_ref, hidden_ref, weight_ref, sent_ref, kept_ref, rows_ref):
    rows = hidden_ref.shape[0] // 4

    @pl.when(pl.program_id(0) == 0)
    def _():
        for i in range(4):
            core = 1 - core_ref[0] if i < 2 else core_ref[0]
            start = (2 * (i % 2) + core) * rows
            rows_ref[i * rows : (i + 1) * rows] = hidden_ref[pl.ds(start, rows), :]

    part = dot(rows_ref[...], weight_ref[...]).astype(bf16)
    sent_ref[...] = part[: 2 * rows]
    kept_ref[...] = part[2 * rows :]


def mixer_parts(hidden, out_weight, core):
    rows, width = hidden.shape
    model = out_weight.shape[1]
    tile = model // 8
    shape = jax.ShapeDtypeStruct((rows // 2, model), bf16)
    spec = pl.BlockSpec((rows // 2, tile), lambda j: (0, j))
    return pl.pallas_call(
        mixer_kernel,
        grid=(model // tile,),
        in_specs=[
            pl.BlockSpec(memory_space=pltpu.SMEM),
            pl.BlockSpec((rows, width), lambda j: (0, 0)),
            pl.BlockSpec((width, tile), lambda j: (0, j)),
        ],
        out_specs=[spec, spec],
        out_shape=[shape, shape],
        scratch_shapes=[pltpu.VMEM((rows, width), bf16)],
        cost_estimate=pl.CostEstimate(
            flops=2 * rows * width * model, bytes_accessed=2 * width * model, transcendentals=0
        ),
        name="mixer",
    )(core, hidden, out_weight)


def pick_kernel(plan, slot_ref, rows_ref, gain_ref, *refs):
    outs, sums = refs[:-1], refs[-1]
    tokens, model = rows_ref.shape
    first, second = slot_ref[0:1, :], slot_ref[1:2, :]
    hits = []
    for blocks in plan:
        for start, size in blocks:
            wanted = start + lax.broadcasted_iota(jnp.int32, (size, tokens), 0)
            hits.append(jnp.where((first == wanted) | (second == wanted), 1.0, 0.0))
    hit = jnp.concatenate(hits, axis=0).astype(bf16)
    square = jnp.zeros((hit.shape[0], 1), f32)
    tile = model // 8
    for j in range(8):
        part = dot(hit, rows_ref[:, j * tile : (j + 1) * tile])
        square += jnp.sum(part * part, axis=1, keepdims=True)
        sums[:, j * tile : (j + 1) * tile] = part
    scale = lax.rsqrt(square / model + epsilon)
    start = 0
    for out_ref, blocks in zip(outs, plan):
        size = sum(n for _, n in blocks)
        out_ref[...] = (
            sums[start : start + size, :] * scale[start : start + size] * gain_ref[...]
        ).astype(bf16)
        start += size


def picked(plan, slot, rows, gain):
    tokens, model = rows.shape
    heights = [sum(n for _, n in blocks) for blocks in plan]
    return pl.pallas_call(
        functools.partial(pick_kernel, plan),
        out_shape=[jax.ShapeDtypeStruct((n, model), bf16) for n in heights],
        scratch_shapes=[pltpu.VMEM((sum(heights), model), f32)],
        cost_estimate=pl.CostEstimate(
            flops=2 * sum(heights) * tokens * model, bytes_accessed=2**23, transcendentals=0
        ),
        name="pick",
    )(slot, rows, gain[None, :])


def inner_kernel(count, *refs):
    parts, weights, out_ref, sums = refs[:count], refs[count:-2], refs[-2], refs[-1]
    step = pl.program_id(0)
    rows = jnp.concatenate([r[...].reshape(-1, r.shape[-1]) for r in parts], axis=0)
    units = weights[0].shape[1]

    @pl.when(step == 0)
    def _():
        sums[...] = jnp.zeros_like(sums)

    for i, w in enumerate(weights):
        sums[:, i * units : (i + 1) * units] += dot(rows, w[...])

    @pl.when(step == pl.num_programs(0) - 1)
    def _():
        gate_val, up_val = sums[:, : 2 * units], sums[:, 2 * units :]
        out_ref[...] = (gate_val / (1.0 + jnp.exp(-gate_val)) * up_val).astype(bf16)


def inner_of(parts, weights, size):
    model, units = weights[0].shape
    depth = model // 4
    height = size * len(parts)
    specs = []
    for array, start in parts:
        if array.ndim == 3:
            spec = pl.BlockSpec((1, size, depth), lambda d, start=start: (start, 0, d))
        else:
            block = start // size
            spec = pl.BlockSpec((size, depth), lambda d, block=block: (block, d))
        specs.append(spec)
    return pl.pallas_call(
        functools.partial(inner_kernel, len(parts)),
        grid=(model // depth,),
        in_specs=specs + [pl.BlockSpec((depth, units), lambda d: (d, 0))] * 4,
        out_specs=pl.BlockSpec((height, 2 * units), lambda d: (0, 0)),
        out_shape=jax.ShapeDtypeStruct((height, 2 * units), bf16),
        scratch_shapes=[pltpu.VMEM((height, 4 * units), f32)],
        cost_estimate=pl.CostEstimate(
            flops=8 * height * model * units,
            bytes_accessed=8 * model * units,
            transcendentals=height * units,
        ),
        name="inner",
    )(*[a for a, _ in parts], *weights)


class Order:
    def __init__(self):
        self.last = None

    def __call__(self, stage, *inputs):
        if self.last is not None:
            inputs, _ = lax.optimization_barrier((inputs, self.last))
        result = stage(*inputs)
        self.last = jax.tree.leaves(result)[0]
        return result


def everything(
    queries,
    key_rows,
    value_rows,
    gate_rows,
    log_decay,
    head_gain,
    out_weight,
    expert_input,
    input_gain,
    route_ids,
    route_weight,
    expert_gate,
    expert_up,
    expert_down,
):
    then = Order()
    tokens, model = expert_input.shape
    ep = lax.axis_size("ep")
    rank, index = lax.axis_index("ep"), lax.axis_index("tp")
    y, z, x, c = rank % 2, rank // 2, index // 2, index % 2
    pairs = ep // 2
    quota = 2 * tokens // pairs // 4
    window = 3 * quota // 4
    units = expert_gate.shape[2]
    half, quarter = model // 2, model // 4
    groups = {
        "a": list(range(pairs // 2)),
        "b": list(range(pairs // 2, 3 * pairs // 4)),
        "c": list(range(3 * pairs // 4, pairs)),
    }
    sides_of = {"a": 2, "b": 1, "c": 1}
    alone = pairs == 4 and window % 16 == 0
    sent_of = groups
    if alone:
        groups, sent_of = {"a": [1], "b": [2], "c": [0, 3]}, {"a": [1], "b": [2], "c": [3]}
    size_of = {g: len(groups[g]) * window for g in groups}

    ids = route_ids.T.reshape(-1)
    one_hot = (ids[:, None] == jnp.arange(ep, dtype=jnp.int32)[None, :]).astype(f32)
    below = jnp.tril(jnp.ones((2 * tokens, 2 * tokens), bf16), -1)
    rank_of = dot(below, one_hot.astype(bf16))
    counts = jnp.sum(one_hot, axis=0)
    base = jnp.where(jnp.arange(ep) % 2 == y, 0.0, counts.reshape(pairs, 2)[:, ::-1].reshape(-1))
    place = jnp.sum(one_hot * (rank_of + base[None, :]), axis=1).astype(jnp.int32)
    turned = (place & 3) ^ index
    slot = (((ids >> 1) ^ z) * 4 + (turned & 1) * 2 + (turned >> 1)) * quota + (place >> 2)
    slot = slot.reshape(2, tokens)
    near_counts = jnp.where(y == 0, counts.reshape(pairs, 2)[:, 0], counts.reshape(pairs, 2)[:, 1])

    def blocks(ks, sides, low, n):
        return [((k * 4 + side) * quota + low, n) for side in range(sides) for k in ks]

    keys = ["c", "b", "a"]
    plan = [blocks(sent_of[g], sides_of[g], 0, quota) for g in keys]
    if alone:
        keys += ["far0", "near0"]
        plan += [blocks([0], 2, quota - window, window), blocks([0], 2, 0, window)]
    rows = dict(zip(keys, then(lambda *v: picked(plan, *v), slot, expert_input, input_gain)))

    def send_z(g):
        ks = sent_of[g]
        if len(ks) == 1:
            return swap(rows[g], "ep", 2 * ks[0])
        parts = rows[g].reshape(sides_of[g], len(ks), quota, model)
        return jnp.stack(
            [parts[:, j] if k == 0 else swap(parts[:, j], "ep", 2 * k) for j, k in enumerate(ks)],
            axis=1,
        )

    landed = {g: send_z(g) for g in ("c", "b", "a")}
    far, near, near_x, far_x = {}, {}, {}, {}
    if alone:
        near["0"], far["0"] = rows["near0"], swap(rows["far0"], "ep", 1)

    gate_own, up_own = expert_gate[0], expert_up[0]
    gate_other, up_other = swap(gate_own, "tp", 1), swap(up_own, "tp", 1)
    weights = (gate_own, gate_other, up_own, up_other)

    cut = lambda a, start, n: lax.dynamic_slice_in_dim(a, start, n, a.ndim - 1)
    down_own = expert_down[0]
    down_x, down_c = then(
        lambda d: (cut(d, (1 - x) * half, half), cut(d, x * half + (1 - c) * quarter, quarter)),
        down_own,
    )
    down_x, down_c = swap(down_x, "tp", 2), swap(down_c, "tp", 1)

    inside, queries_turned, state, decay, sent = then(
        retention_inside, queries, key_rows, value_rows, log_decay
    )
    got = swap(sent, "ep", 1)
    links = (state, decay)
    combine_step = 1

    def run_combine():
        nonlocal links, got, combine_step
        late = jnp.where((rank & combine_step) > 0, 1, 0).astype(jnp.int32).reshape(1)
        final = 2 * combine_step >= ep
        out = then(lambda *v: combine(final, *v), late, got, *links)
        combine_step *= 2
        if final:
            return out[0]
        links = (out[2], out[3], out[0], out[1])
        got = swap(out[4], "ep", combine_step)

    def split_rows(g):
        def stage(v):
            v = v.reshape(sides_of[g], -1, quota, model)
            f = v[:, :, quota - window :].reshape(-1, model)
            if alone and sides_of[g] == 2:
                return f, v[:, 0]
            return f, v[:, :, :window].reshape(-1, model)

        f, near[g] = then(stage, landed[g])
        far[g] = swap(f, "ep", 1)
        if sides_of[g] == 1:
            near_x[g] = swap(near[g], "tp", 2)

    def send_far(g):
        (f,) = then(lambda f: (f,), far[g])
        far[g], far_x[g] = f, swap(f, "tp", 2)

    inner, got_x, both, got_c = {}, {}, {}, {}

    def run_inner(g):
        parts, size = [], window if alone else size_of[g]
        for part, part_x in ((near, near_x), (far, far_x)):
            for side in range(2):
                if 0 in groups[g] and alone:
                    parts.append((part["0"], side * size))
                if sides_of[g] == 1:
                    parts.append(((part, part_x)[side][g], 0))
                else:
                    parts.append((part[g], side if part[g].ndim == 3 else side * size))
        starts = [start for _, start in parts]
        inner[g] = then(
            lambda *v: inner_of(list(zip(v, starts)), v[len(starts) :], size),
            *[p for p, _ in parts],
            *weights,
        )
        got_x[g] = swap(inner[g], "tp", 2)

    def run_both(g):
        def stage(own, other):
            other = other.reshape(2, 2, size_of[g], 2 * units)
            other = jnp.stack([other[:, 1], other[:, 0]], axis=1).reshape(own.shape)
            flip = [own[:, units:], own[:, :units], other[:, units:], other[:, :units]]
            return jnp.concatenate(flip, axis=1), jnp.concatenate([own, other], axis=1)

        flipped, both[g] = then(stage, inner[g], got_x[g])
        got_c[g] = swap(flipped, "tp", 1)

    result, result_far, back = {}, {}, {}

    def run_down(g):
        def rows_of(a, b, part):
            kept = slice(part * 2 * size_of[g], (part + 1) * 2 * size_of[g])
            return jnp.concatenate([a[kept], b[kept]], axis=0)

        out = then(lambda a, b, d: dot(rows_of(a, b, 1), d).astype(bf16), both[g], got_c[g], down)
        result_far[g] = swap(out, "ep", 1)
        result[g] = then(
            lambda a, b, d: dot(rows_of(a, b, 0), d).astype(bf16), both[g], got_c[g], down
        )

    def run_merge(g):
        ks = groups[g]

        def stage(n, f, l):
            n = n.reshape(2, 2, len(ks), window, quarter)
            f = f.reshape(2, 2, len(ks), window, quarter)
            pad = [(0, 0)] * 5
            pad[3] = (0, quota - window)
            n = jnp.pad(n, pad)
            pad[3] = (quota - window, 0)
            f = jnp.pad(f, pad)
            spot = lax.broadcasted_iota(f32, (2, 2, len(ks), quota, 1), 3)
            merged = jnp.where(spot < l[:, :, :, None, None], n, f)
            return [merged[:, :, j].reshape(4 * quota, quarter) for j in range(len(ks))]

        parts = then(stage, result[g], result_far[g], jnp.stack([limits[:, :, k] for k in ks], axis=2))
        for part, k in zip(parts, ks):
            back[k] = part if k == 0 else swap(part, "ep", 2 * k)

    def run_total(ks, total):
        def stage(slots, weight, total, *parts):
            for part, k in zip(parts, ks):
                places = k * 4 * quota + jnp.arange(4 * quota, dtype=jnp.int32)[None, :]
                mix = jnp.where(slots[0][:, None] == places, weight[:, :1], 0.0)
                mix += jnp.where(slots[1][:, None] == places, weight[:, 1:], 0.0)
                total = dot(mix.astype(bf16), part) + (0.0 if total is None else total)
            return total

        return then(stage, slot, route_weight, total, *[back[k] for k in ks])

    def half_rows(side):
        def stage(a, b):
            pick = lambda v: lax.dynamic_slice_in_dim(v, side * (tokens // 4), tokens // 4, 0)
            return pick(a).astype(f32) + pick(b).astype(f32)

        return stage

    split_rows("c")
    while 4 * combine_step < ep:
        run_combine()
    known = [near_counts] + [swap(near_counts, "ep", 2 * k) for k in range(1, pairs)]
    (down_c2,) = then(lambda d: (cut(d, (1 - c) * quarter, quarter),), down_x)
    down_c2 = swap(down_c2, "tp", 1)
    send_far("c")

    def build_down(own, x_got, c_got, c_got2):
        parts = [cut(own, index * quarter, quarter), c_got, cut(x_got, c * quarter, quarter), c_got2]
        return jnp.concatenate(parts, axis=0)

    down = then(build_down, down_own, down_x, down_c, down_c2)
    split_rows("b")
    run_inner("c")
    send_far("b")
    split_rows("a")
    run_both("c")

    def limits_of(known):
        turn_of = ((jnp.arange(2)[None, :] * 2 + jnp.arange(2)[:, None]) ^ index).astype(f32)
        numbers = lax.dynamic_slice_in_dim(jnp.stack(known), z, 1, 1)[:, 0]
        return jnp.ceil((numbers[None, None, :] - turn_of[:, :, None]) / 4)

    limits = then(limits_of, known)
    run_down("c")
    run_combine()
    run_inner("b")
    run_merge("c")
    incoming = run_combine()
    hidden = then(retention_outside, inside, queries_turned, incoming, gate_rows, head_gain)
    run_both("b")
    run_inner("a")
    run_down("b")
    mix_sent, mix_kept = then(mixer_parts, hidden, out_weight, c.astype(jnp.int32).reshape(1))
    mix_got = swap(mix_sent, "tp", 1)
    run_both("a")
    run_merge("b")
    run_down("a")
    mix_far = swap(
        then(lambda a, b: half_rows(1 - x)(a, b).astype(bf16), mix_kept, mix_got), "tp", 2
    )
    run_merge("a")
    total = run_total(groups["c"], None)
    mixer_out = then(
        lambda a, b, f: (half_rows(x)(a, b) + f.astype(f32)).astype(bf16), mix_kept, mix_got, mix_far
    )
    total = run_total(groups["a"], total)
    total = run_total(groups["b"], total)
    return (mixer_out, total.astype(bf16))


def solution(mesh):
    assert mesh.shape["tp"] == 4 and mesh.shape["ep"] & (mesh.shape["ep"] - 1) == 0
    placed = (
        P("ep", "tp"),
        P("ep", "tp"),
        P("ep", "tp"),
        P("ep", "tp"),
        P("tp", "ep"),
        P("tp"),
        P("tp", None),
        P("ep", None),
        P(),
        P("ep", None),
        P("ep", None),
        P("ep", None, "tp"),
        P("ep", None, "tp"),
        P("ep", "tp", None),
    )
    return jax.shard_map(
        everything,
        mesh=mesh,
        in_specs=placed,
        out_specs=(P(("ep", "tp"), None), P("ep", "tp")),
        check_vma=False,
    )
```

time: 511 us -> 239 us (0.47); the launches traced: 503 us -> 238 us
  blocking collectives: 151 us -> 0 us
  local copies, waits for them, and re-layouts: 97 us -> 12.4 us
  Pallas kernels: 0 us -> 57.4 us
  matrix products: 56.1 us -> 13.4 us
  other arithmetic: 40.3 us -> 10.5 us
  waiting for transfers between devices: 132 us -> 104 us
  starting transfers between devices: 11.4 us -> 38.4 us
  between operations: 15.4 us -> 1.47 us
    ppermute x0 -> x36, waiting for transfers between devices: none -> 104 us  [swap(): return lax.ppermute(value, axis, [(i, i ^ mask) for i in range(size)])]
    all_gather x4 -> x0, waiting for transfers between devices: 93.2 us -> none  [the longest x1 51.3 us: body(): lax.all_gather(expert_down, 'tp', axis=1, tiled=True)]
    all_to_all x1 -> x0, blocking collectives: 76.6 us -> none  [body(): lax.all_to_all(finished, 'ep', split_axis=0, concat_axis=0, tiled=True)]
    unnamed x1 -> x0, blocking collectives: 74.5 us -> none
    pallas_call x0 -> x10, Pallas kernels: none -> 57.4 us  [the longest x3 20.6 us: inner_of(): pl.pallas_call(functools.partial(inner_kernel, len(parts)), grid=(model /...]
    dot_general x8 -> x11, matrix products: 56.1 us -> 13.4 us  [dot(): return jnp.dot(a, b, preferred_element_type=f32)]
    ppermute x0 -> x36, starting transfers between devices: none -> 38.4 us  [swap(): return lax.ppermute(value, axis, [(i, i ^ mask) for i in range(size)])]
    all_to_all x2 -> x0, waiting for transfers between devices: 36.7 us -> none  [the longest x1 36.7 us: body(): lax.all_to_all(came_back, 'tp', split_axis=3, concat_axis=2, tiled=True)]
  transfers between devices with their start and end apart: 7 -> 36, of which waited for: 3 -> 14; matrix products, arithmetic and copies ran while one was open for 35% -> 12% of each run, Pallas kernels for 0% -> 21%
where the time goes in v1:
time: 239 us; the launch traced here: 238 us
  waiting for transfers between devices  104 us (44%)
  Pallas kernels  57.4 us (24%)
  starting transfers between devices  38.4 us (16%)
  matrix products  13.4 us (6%)
  local copies, waits for them, and re-layouts  12.4 us (5%)
  other arithmetic  10.5 us (4%)
    ppermute x36, waiting for transfers between devices, swap(): return lax.ppermute(value, axis, [(i, i ^ mask) for i in range(size)])  104 us
    ppermute x36, starting transfers between devices, swap(): return lax.ppermute(value, axis, [(i, i ^ mask) for i in range(size)])  38.4 us
    pallas_call x3, Pallas kernels, inner_of(): pl.pallas_call(functools.partial(inner_kernel, len(parts)), grid=(model /...  20.6 us
    dot_general x11, matrix products, dot(): return jnp.dot(a, b, preferred_element_type=f32)  13.4 us
    pallas_call x1, Pallas kernels, mixer_parts(): pl.pallas_call(mixer_kernel, grid=(model // tile,), in_specs=[pl.BlockSpe...  10.3 us
    pallas_call x1, Pallas kernels, retention_inside(): pl.pallas_call(inside_kernel, grid=(heads,), in_specs=[cols(width), cols(...  8.17 us
    pallas_call x3, Pallas kernels, combine(): pl.pallas_call(combine_kernel, in_specs=[pl.BlockSpec(memory_space=pltpu....  6.89 us
    pallas_call x1, Pallas kernels, picked(): pl.pallas_call(functools.partial(pick_kernel, plan), out_shape=[jax.Shape...  6.44 us
  transfers between devices with their start and end apart: 36, of which 14 were waited for; matrix products, arithmetic and copies ran while one was open for 12% of the time, Pallas kernels for 21%

profile of v1, /device:TPU:0, one launch (start us, length us, event | category | flops | bytes accessed | tf_op | source)
XLA Modules:
  0.0 238.0 jit_solution(11928421142086259723)
XLA Ops:
  3.3 6.4 %pick.1 = (bf16[64,4096]{1,0:T(8,128)(2,1)}, bf16[64,4096]{1,0:T(8,128)(2,1)}, bf16[128,4096]{1,0:T(8,128)(2,1)}, bf16[96,4096]{1,0:T(8,128)(2,1)}, bf16[96,4096]{1,0:T(8,128)(2,1)}) custom-call(s32[2,512]{1,0:T(2,128)} %multiply_add_fusion.slot_ref, bf16[512,4096]{1,0:T(8,128)(2,1)} %rows_ref.1, f32[1,4096]{1,0:T(1,128)} %bitcast.140), custom_call_target="tpu_custom_call" | custom-call | flops 1879048192 | bytes 8388608 | tf_op jit(solution)/shard_map/pick/pallas_call | solution.py:282
  9.8 5.1 %collective-permute-start.1 = (bf16[64,4096]{1,0:T(8,128)(2,1)}, bf16[64,4096]{1,0:T(8,128)(2,1)S(1)}, u32[]{:S(2)}, u32[]{:S(2)}) collective-permute-start(bf16[64,4096]{1,0:T(8,128)(2,1)} %get-tuple-element.145), channel_id=1, source_target_pairs={{0,24},{4,28},{8,16},{12,20},{16,8},{20,12},{24,0},{28,4},{1,25},{... | collective-permute-start | bytes 1572872 | tf_op jit(solution)/shard_map/ppermute | solution.py:18
  15.9 1.5 collective-permute-start.6
  19.5 8.2 %inside.1 = (f32[512,1024]{1,0:T(8,128)}, f32[512,512]{1,0:T(8,128)}, f32[4,128,256]{2,1,0:T(8,128)}, f32[4,8,256]{2,1,0:T(8,128)}, bf16[4,144,256]{2,1,0:T(8,128)(2,1)}) custom-call(bf16[512,512]{1,0:T(8,128)(2,1)} %q_ref, bf16[512,512]{1,0:T(8,128)(2,1)} %k_ref, bf16[512,1024]{1,0:T(8,128)(2,1)} %v_ref, f32[512,128]{1,0:T(8,128)} %get-tuple-element.334.cos_ref, ...), custom_call_target="tpu_custom_call" | custom-call | flops 2147483648 | bytes 8388608 | tf_op jit(solution)/shard_map/inside/pallas_call | solution.py:163
  27.7 1.6 collective-permute-start
  30.8 5.5 %collective-permute-done.got_ref = bf16[4,144,256]{2,1,0:T(8,128)(2,1)} collective-permute-done((bf16[4,144,256]{2,1,0:T(8,128)(2,1)}, bf16[4,144,256]{2,1,0:T(8,128)(2,1)}, u32[]{:S(2)}, u32[]{:S(2)}) %collective-permute-start) | collective-permute-done | bytes 294944 | tf_op jit(solution)/shard_map/ppermute | solution.py:18
  36.2 2.3 combine.3
  38.5 2.4 %collective-permute-done.6 = bf16[256,2048]{1,0:T(8,128)(2,1)} collective-permute-done((bf16[256,2048]{1,0:T(8,128)(2,1)}, bf16[256,2048]{1,0:T(8,128)(2,1)}, u32[]{:S(2)}, u32[]{:S(2)}) %collective-permute-start.6) | collective-permute-done | bytes 1048608 | tf_op jit(solution)/shard_map/ppermute | solution.py:18
  42.0 1.6 collective-permute-start.5
  44.1 10.3 %collective-permute-done.5.refs_5_ = bf16[48,4096]{1,0:T(8,128)(2,1)} collective-permute-done((bf16[48,4096]{1,0:T(8,128)(2,1)}, bf16[48,4096]{1,0:T(8,128)(2,1)}, u32[]{:S(2)}, u32[]{:S(2)}) %collective-permute-start.5) | collective-permute-done | bytes 393248 | tf_op jit(solution)/shard_map/ppermute | solution.py:18
  54.4 1.8 collective-permute-start.10
  57.3 2.8 %pad_maximum_fusion = bf16[1024,1024]{1,0:T(8,128)(2,1)} fusion(bf16[256,1024]{1,0:T(8,128)(2,1)} %collective-permute-done.12, bf16[256,1024]{1,0:T(8,128)(2,1)S(1)} %constant_dynamic-slice_fusion.1, bf16[256,1024]{1,0:T(8,128)(2,1)} %collective-permute-done.11, bf16[256,1024]{1,0:T(8,128)(2,1)S(1)} %constant_dynamic-slice_fusion.2), kind=kLoop, calls=%fused_computation.3 | loop fusion | flops 8388608 | bytes 4194304 | tf_op jit(solution)/shard_map/concatenate | solution.py:564
  60.1 19.2 %collective-permute-done.10 = bf16[64,4096]{1,0:T(8,128)(2,1)} collective-permute-done((bf16[64,4096]{1,0:T(8,128)(2,1)}, bf16[64,4096]{1,0:T(8,128)(2,1)}, u32[]{:S(2)}, u32[]{:S(2)}) %collective-permute-start.10) | collective-permute-done | bytes 524320 | tf_op jit(solution)/shard_map/ppermute | solution.py:18
  79.3 1.5 collective-permute-start.3
  81.3 1.2 slice_bitcast_fusion
  82.6 8.7 %collective-permute-done.3.refs_3_ = bf16[48,4096]{1,0:T(8,128)(2,1)S(1)} collective-permute-done((bf16[48,4096]{1,0:T(8,128)(2,1)S(1)}, bf16[48,4096]{1,0:T(8,128)(2,1)S(1)}, u32[]{:S(2)}, u32[]{:S(2)}) %collective-permute-start.3) | collective-permute-done | bytes 393248 | tf_op jit(solution)/shard_map/ppermute | solution.py:18
  91.3 1.5 collective-permute-start.15
  92.8 5.9 %collective-permute-done.7.refs_7_ = bf16[48,4096]{1,0:T(8,128)(2,1)S(1)} collective-permute-done((bf16[48,4096]{1,0:T(8,128)(2,1)}, bf16[48,4096]{1,0:T(8,128)(2,1)S(1)}, u32[]{:S(2)}, u32[]{:S(2)}) %collective-permute-start.7) | collective-permute-done | bytes 393248 | tf_op jit(solution)/shard_map/ppermute | solution.py:18
  99.5 8.0 %inner.3 = bf16[384,512]{1,0:T(8,128)(2,1)} custom-call(bf16[96,4096]{1,0:T(8,128)(2,1)} %get-tuple-element.178.refs_0_.refs_2_, bf16[48,4096]{1,0:T(8,128)(2,1)} %copy-done.14, bf16[96,4096]{1,0:T(8,128)(2,1)} %get-tuple-element.178.refs_0_.refs_2_, bf16[48,4096]{1,0:T(8,128)(2,1)} %copy-done.16, bf16[96,4096]{1,0:T(8,128)(2,1)} %collective-permute-done.4.refs_4_.refs_6_, ...), custom_call_target="tpu_custom_call" | custom-call | flops 3221225472 | bytes 8388608 | tf_op jit(solution)/shard_map/inner/pallas_call | solution.py:324
  107.5 1.6 collective-permute-start.13
  109.4 4.3 %collective-permute-start.19 = (f32[4]{0:T(128)S(1)}, f32[4]{0:T(128)S(1)}, u32[]{:S(2)}, u32[]{:S(2)}) collective-permute-start(f32[4]{0:T(128)S(1)} %select_reduce_fusion), channel_id=1, source_target_pairs={{0,24},{4,28},{8,16},{12,20},{16,8},{20,12},{24,0},{28,4},{1,25},{... | collective-permute-start | bytes 56 | tf_op jit(solution)/shard_map/ppermute | solution.py:18
  114.7 3.2 %collective-permute-done.13 = bf16[384,512]{1,0:T(8,128)(2,1)S(1)} collective-permute-done((bf16[384,512]{1,0:T(8,128)(2,1)}, bf16[384,512]{1,0:T(8,128)(2,1)S(1)}, u32[]{:S(2)}, u32[]{:S(2)}) %collective-permute-start.13) | collective-permute-done | bytes 393248 | tf_op jit(solution)/shard_map/ppermute | solution.py:18
  118.9 1.6 collective-permute-start.22
  120.9 1.9 convolution_convert_fusion.1
  122.8 1.5 collective-permute-start.21
  126.1 1.9 convolution_convert_fusion
  127.9 2.5 %combine.4 = (f32[4,128,256]{2,1,0:T(8,128)}, f32[4,8,256]{2,1,0:T(8,128)}, f32[4,128,256]{2,1,0:T(8,128)}, f32[4,8,256]{2,1,0:T(8,128)}, bf16[4,144,256]{2,1,0:T(8,128)(2,1)}) custom-call(s32[1]{0:T(128)} %bitcast.4.late_ref, bf16[4,144,256]{2,1,0:T(8,128)(2,1)} %collective-permute-done.2.got_ref, f32[4,128,256]{2,1,0:T(8,128)} %get-tuple-element.205.s_ref, ...), custom_call_target="tpu_custom_call" | custom-call | tf_op jit(solution)/shard_map/combine/pallas_call | solution.py:140
  131.0 7.4 %collective-permute-done.23.refs_3_ = bf16[48,4096]{1,0:T(8,128)(2,1)} collective-permute-done((bf16[48,4096]{1,0:T(8,128)(2,1)S(1)}, bf16[48,4096]{1,0:T(8,128)(2,1)}, u32[]{:S(2)}, u32[]{:S(2)}) %collective-permute-start.23) | collective-permute-done | bytes 393248 | tf_op jit(solution)/shard_map/ppermute | solution.py:18
  138.5 6.3 %inner.4 = bf16[192,512]{1,0:T(8,128)(2,1)} custom-call(bf16[48,4096]{1,0:T(8,128)(2,1)} %copy-done.13, bf16[48,4096]{1,0:T(8,128)(2,1)} %collective-permute-done.22.refs_1_, bf16[48,4096]{1,0:T(8,128)(2,1)} %copy-done.15, bf16[48,4096]{1,0:T(8,128)(2,1)} %collective-permute-done.23.refs_3_, bf16[4096,256]{1,0:T(8,128)(2,1)} %bitcast.85, ...), custom_call_target="tpu_custom_call" | custom-call | flops 1610612736 | bytes 8388608 | tf_op jit(solution)/shard_map/inner/pallas_call | solution.py:324
  144.8 1.5 collective-permute-start.24
  146.4 1.4 pad_select_fusion
  148.0 6.0 %collective-permute-done.20.got_ref = bf16[4,144,256]{2,1,0:T(8,128)(2,1)} collective-permute-done((bf16[4,144,256]{2,1,0:T(8,128)(2,1)}, bf16[4,144,256]{2,1,0:T(8,128)(2,1)}, u32[]{:S(2)}, u32[]{:S(2)}) %collective-permute-start.20) | collective-permute-done | bytes 294944 | tf_op jit(solution)/shard_map/ppermute | solution.py:18
  154.0 2.1 combine.5.s_ref
  156.2 5.1 %outside.1.hidden_ref = bf16[512,1024]{1,0:T(8,128)(2,1)} custom-call(f32[512,1024]{1,0:T(8,128)} %get-tuple-element.231.o_ref, f32[512,512]{1,0:T(8,128)} %get-tuple-element.232.qd_ref, f32[4,128,256]{2,1,0:T(8,128)} %combine.5.s_ref, bf16[512,1024]{1,0:T(8,128)(2,1)} %gate_ref, f32[1,1024]{1,0:T(1,128)} %bitcast.133), custom_call_target="tpu_custom_call" | custom-call | flops 536870912 | bytes 4194304 | tf_op jit(solution)/shard_map/outside/pallas_call | solution.py:195
  162.9 6.3 %inner.5 = bf16[192,512]{1,0:T(8,128)(2,1)} custom-call(bf16[2,64,4096]{2,1,0:T(8,128)(2,1)} %bitcast.92, bf16[2,64,4096]{2,1,0:T(8,128)(2,1)} %bitcast.93, bf16[96,4096]{1,0:T(8,128)(2,1)} %copy-done.4, bf16[96,4096]{1,0:T(8,128)(2,1)} %copy-done.4, bf16[4096,256]{1,0:T(8,128)(2,1)} %bitcast.86, bf16[4096,256]{1,0:T(8,128)(2,1)} %collective-permute-done.8.refs_9_.refs_5_, ...), custom_call_target="tpu_custom_call" | custom-call | flops 1610612736 | bytes 8388608 | tf_op jit(solution)/shard_map/inner/pallas_call | solution.py:324
  169.2 1.5 collective-permute-start.28
  172.6 2.9 %convolution_convert_fusion.5 = bf16[192,1024]{1,0:T(8,128)(2,1)} fusion(bf16[1024,1024]{1,0:T(8,128)(2,1)} %pad_maximum_fusion, bf16[96,1024]{1,0:T(8,128)(2,1)S(1)} %slice.196, bf16[96,1024]{1,0:T(8,128)(2,1)S(1)} %slice.195), kind=kOutput, calls=%fused_computation.15 | convolution fusion | flops 403636224 | bytes 2883584 | tf_op jit(solution)/shard_map/dot_general | solution.py:22
  175.6 1.3 convolution_convert_fusion.4
  176.9 10.3 %mixer.1 = (bf16[256,4096]{1,0:T(8,128)(2,1)}, bf16[256,4096]{1,0:T(8,128)(2,1)}) custom-call(s32[1]{0:T(128)} %bitcast.26.core_ref, bf16[512,1024]{1,0:T(8,128)(2,1)} %outside.1.hidden_ref, bf16[1024,4096]{1,0:T(8,128)(2,1)} %weight_ref), custom_call_target="tpu_custom_call" | custom-call | flops 4294967296 | bytes 8388608 | tf_op jit(solution)/shard_map/mixer/pallas_call | solution.py:235
  188.5 1.5 collective-permute-start.30
  190.3 9.4 %collective-permute-done.30 = bf16[192,1024]{1,0:T(8,128)(2,1)S(1)} collective-permute-done((bf16[192,1024]{1,0:T(8,128)(2,1)}, bf16[192,1024]{1,0:T(8,128)(2,1)S(1)}, u32[]{:S(2)}, u32[]{:S(2)}) %collective-permute-start.30) | collective-permute-done | bytes 393248 | tf_op jit(solution)/shard_map/ppermute | solution.py:18
  200.7 1.6 collective-permute-start.33
  203.9 7.1 %collective-permute-done.33 = bf16[192,1024]{1,0:T(8,128)(2,1)S(1)} collective-permute-done((bf16[192,1024]{1,0:T(8,128)(2,1)S(1)}, bf16[192,1024]{1,0:T(8,128)(2,1)S(1)}, u32[]{:S(2)}, u32[]{:S(2)}) %collective-permute-start.33) | collective-permute-done | bytes 393248 | tf_op jit(solution)/shard_map/ppermute | solution.py:18
  211.2 3.1 %collective-permute-start.34 = (bf16[256,1024]{1,0:T(8,128)(2,1)S(1)}, bf16[256,1024]{1,0:T(8,128)(2,1)S(1)}, u32[]{:S(2)}, u32[]{:S(2)}) collective-permute-start(bf16[256,1024]{1,0:T(8,128)(2,1)S(1)} %bitcast.105), channel_id=1, source_target_pairs={{0,8},{4,12},{8,0},{12,4},{16,24},{20,28},{24,16},{28,20},{1,9},{5... | collective-permute-start | bytes 1572872 | tf_op jit(solution)/shard_map/ppermute | solution.py:18
  215.6 11.6 %collective-permute-done.31 = bf16[128,4096]{1,0:T(8,128)(2,1)S(1)} collective-permute-done((bf16[128,4096]{1,0:T(8,128)(2,1)S(1)}, bf16[128,4096]{1,0:T(8,128)(2,1)S(1)}, u32[]{:S(2)}, u32[]{:S(2)}) %collective-permute-start.31) | collective-permute-done | bytes 1048608 | tf_op jit(solution)/shard_map/ppermute | solution.py:18
  227.3 1.5 add_convert_fusion.1
  228.7 7.0 %collective-permute-done.34 = bf16[256,1024]{1,0:T(8,128)(2,1)S(1)} collective-permute-done((bf16[256,1024]{1,0:T(8,128)(2,1)S(1)}, bf16[256,1024]{1,0:T(8,128)(2,1)S(1)}, u32[]{:S(2)}, u32[]{:S(2)}) %collective-permute-start.34) | collective-permute-done | bytes 524320 | tf_op jit(solution)/shard_map/ppermute | solution.py:18
  236.4 1.6 add_convert_fusion
  (178 shorter events, 26.2 us)
Async XLA Ops:
  0.6 14.2 %copy-start = (bf16[1,256,4096]{2,1,0:T(8,128)(2,1)S(1)}, bf16[1,256,4096]{2,1,0:T(8,128)(2,1)}, u32[]{:S(2)}) copy-start(bf16[1,256,4096]{2,1,0:T(8,128)(2,1)} %param.27) | copy-start | bytes 6291460
  9.8 20.1 %collective-permute-start.1 = (bf16[64,4096]{1,0:T(8,128)(2,1)}, bf16[64,4096]{1,0:T(8,128)(2,1)S(1)}, u32[]{:S(2)}, u32[]{:S(2)}) collective-permute-start(bf16[64,4096]{1,0:T(8,128)(2,1)} %get-tuple-element.145), channel_id=1, source_target_pairs={{0,24},{4,28},{8,16},{12,20},{16,8},{20,12},{24,0},{28,4},{1,25},{... | collective-permute-start | bytes 1572872 | tf_op jit(solution)/shard_map/ppermute | solution.py:18
  15.9 24.9 %collective-permute-start.6 = (bf16[256,2048]{1,0:T(8,128)(2,1)}, bf16[256,2048]{1,0:T(8,128)(2,1)}, u32[]{:S(2)}, u32[]{:S(2)}) collective-permute-start(bf16[256,2048]{1,0:T(8,128)(2,1)} %constant_dynamic-slice_fusion.5), channel_id=1, source_target_pairs={{0,2},{1,3},{2,0},{3,1},{4,6},{5,7},{6,4},{7,5},{8,10},{9,11},{10,... | collective-permute-start | bytes 3145736 | tf_op jit(solution)/shard_map/ppermute | solution.py:18
  27.7 8.6 %collective-permute-start = (bf16[4,144,256]{2,1,0:T(8,128)(2,1)}, bf16[4,144,256]{2,1,0:T(8,128)(2,1)}, u32[]{:S(2)}, u32[]{:S(2)}) collective-permute-start(bf16[4,144,256]{2,1,0:T(8,128)(2,1)} %get-tuple-element.153), channel_id=1, source_target_pairs={{0,4},{4,0},{8,12},{12,8},{16,20},{20,16},{24,28},{28,24},{1,5},{5... | collective-permute-start | bytes 884744 | tf_op jit(solution)/shard_map/ppermute | solution.py:18
  29.3 14.3 %collective-permute-start.11 = (bf16[256,1024]{1,0:T(8,128)(2,1)S(1)}, bf16[256,1024]{1,0:T(8,128)(2,1)}, u32[]{:S(2)}, u32[]{:S(2)}) collective-permute-start(bf16[256,1024]{1,0:T(8,128)(2,1)S(1)} %constant_dynamic-slice_fusion.3), channel_id=1, source_target_pairs={{0,1},{1,0},{2,3},{3,2},{4,5},{5,4},{6,7},{7,6},{8,9},{9,8},{10,11... | collective-permute-start | bytes 1572872 | tf_op jit(solution)/shard_map/ppermute | solution.py:18
  29.4 69.3 %collective-permute-start.8 = (bf16[4096,256]{1,0:T(8,128)(2,1)}, bf16[4096,256]{1,0:T(8,128)(2,1)}, u32[]{:S(2)}, u32[]{:S(2)}) collective-permute-start(bf16[4096,256]{1,0:T(8,128)(2,1)} %bitcast.83), channel_id=1, source_target_pairs={{0,1},{1,0},{2,3},{3,2},{4,5},{5,4},{6,7},{7,6},{8,9},{9,8},{10,11... | collective-permute-start | bytes 6291464 | tf_op jit(solution)/shard_map/ppermute | solution.py:18
  29.9 68.9 %collective-permute-start.9 = (bf16[4096,256]{1,0:T(8,128)(2,1)}, bf16[4096,256]{1,0:T(8,128)(2,1)}, u32[]{:S(2)}, u32[]{:S(2)}) collective-permute-start(bf16[4096,256]{1,0:T(8,128)(2,1)} %bitcast.87), channel_id=1, source_target_pairs={{0,1},{1,0},{2,3},{3,2},{4,5},{5,4},{6,7},{7,6},{8,9},{9,8},{10,11... | collective-permute-start | bytes 6291464 | tf_op jit(solution)/shard_map/ppermute | solution.py:18
  30.8 48.5 %copy-start.14 = (bf16[48,4096]{1,0:T(8,128)(2,1)}, bf16[48,4096]{1,0:T(8,128)(2,1)S(1)}, u32[]{:S(2)}) copy-start(bf16[48,4096]{1,0:T(8,128)(2,1)S(1)} %get-tuple-element.177.refs_1_) | copy-start | bytes 1179652
  42.0 14.2 %collective-permute-start.12 = (bf16[256,1024]{1,0:T(8,128)(2,1)S(1)}, bf16[256,1024]{1,0:T(8,128)(2,1)}, u32[]{:S(2)}, u32[]{:S(2)}) collective-permute-start(bf16[256,1024]{1,0:T(8,128)(2,1)S(1)} %constant_dynamic-slice_fusion.4), channel_id=1, source_target_pairs={{0,1},{1,0},{2,3},{3,2},{4,5},{5,4},{6,7},{7,6},{8,9},{9,8},{10,11... | collective-permute-start | bytes 1572872 | tf_op jit(solution)/shard_map/ppermute | solution.py:18
  42.0 12.4 %collective-permute-start.5 = (bf16[48,4096]{1,0:T(8,128)(2,1)}, bf16[48,4096]{1,0:T(8,128)(2,1)}, u32[]{:S(2)}, u32[]{:S(2)}) collective-permute-start(bf16[48,4096]{1,0:T(8,128)(2,1)} %get-tuple-element.293), channel_id=1, source_target_pairs={{0,4},{4,0},{8,12},{12,8},{16,20},{20,16},{24,28},{28,24},{1,5},{5... | collective-permute-start | bytes 1179656 | tf_op jit(solution)/shard_map/ppermute | solution.py:18
  43.6 37.2 %collective-permute-start.4 = (bf16[96,4096]{1,0:T(8,128)(2,1)}, bf16[96,4096]{1,0:T(8,128)(2,1)}, u32[]{:S(2)}, u32[]{:S(2)}) collective-permute-start(bf16[96,4096]{1,0:T(8,128)(2,1)} %get-tuple-element.167), channel_id=1, source_target_pairs={{0,4},{4,0},{8,12},{12,8},{16,20},{20,16},{24,28},{28,24},{1,5},{5... | collective-permute-start | bytes 2359304 | tf_op jit(solution)/shard_map/ppermute | solution.py:18
  54.4 24.9 %collective-permute-start.10 = (bf16[64,4096]{1,0:T(8,128)(2,1)}, bf16[64,4096]{1,0:T(8,128)(2,1)}, u32[]{:S(2)}, u32[]{:S(2)}) collective-permute-start(bf16[64,4096]{1,0:T(8,128)(2,1)} %get-tuple-element.170), channel_id=1, source_target_pairs={{0,16},{4,20},{8,24},{12,28},{16,0},{20,4},{24,8},{28,12},{1,17},{... | collective-permute-start | bytes 1572872 | tf_op jit(solution)/shard_map/ppermute | solution.py:18
  56.2 57.5 %collective-permute-start.14 = (bf16[128,4096]{1,0:T(8,128)(2,1)}, bf16[128,4096]{1,0:T(8,128)(2,1)S(1)}, u32[]{:S(2)}, u32[]{:S(2)}) collective-permute-start(bf16[128,4096]{1,0:T(8,128)(2,1)} %get-tuple-element.188), channel_id=1, source_target_pairs={{0,8},{4,12},{8,0},{12,4},{16,24},{20,28},{24,16},{28,20},{1,9},{5... | collective-permute-start | bytes 3145736 | tf_op jit(solution)/shard_map/ppermute | solution.py:18
  79.3 12.0 %collective-permute-start.3 = (bf16[48,4096]{1,0:T(8,128)(2,1)S(1)}, bf16[48,4096]{1,0:T(8,128)(2,1)S(1)}, u32[]{:S(2)}, u32[]{:S(2)}) collective-permute-start(bf16[48,4096]{1,0:T(8,128)(2,1)S(1)} %get-tuple-element.177.refs_1_), channel_id=1, source_target_pairs={{0,2},{1,3},{2,0},{3,1},{4,6},{5,7},{6,4},{7,5},{8,10},{9,11},{10,... | collective-permute-start | bytes 1179656 | tf_op jit(solution)/shard_map/ppermute | solution.py:18
  80.8 17.9 %collective-permute-start.7 = (bf16[48,4096]{1,0:T(8,128)(2,1)}, bf16[48,4096]{1,0:T(8,128)(2,1)S(1)}, u32[]{:S(2)}, u32[]{:S(2)}) collective-permute-start(bf16[48,4096]{1,0:T(8,128)(2,1)} %collective-permute-done.5.refs_5_), channel_id=1, source_target_pairs={{0,2},{1,3},{2,0},{3,1},{4,6},{5,7},{6,4},{7,5},{8,10},{9,11},{10,... | collective-permute-start | bytes 1179656 | tf_op jit(solution)/shard_map/ppermute | solution.py:18
  82.5 36.3 %copy-start.13 = (bf16[48,4096]{1,0:T(8,128)(2,1)}, bf16[48,4096]{1,0:T(8,128)(2,1)S(1)}, u32[]{:S(2)}) copy-start(bf16[48,4096]{1,0:T(8,128)(2,1)S(1)} %get-tuple-element.214.refs_0_) | copy-start | bytes 1179652
  91.3 18.1 %collective-permute-start.15 = (bf16[48,4096]{1,0:T(8,128)(2,1)S(1)}, bf16[48,4096]{1,0:T(8,128)(2,1)S(1)}, u32[]{:S(2)}, u32[]{:S(2)}) collective-permute-start(bf16[48,4096]{1,0:T(8,128)(2,1)S(1)} %get-tuple-element.291), channel_id=1, source_target_pairs={{0,4},{4,0},{8,12},{12,8},{16,20},{20,16},{24,28},{28,24},{1,5},{5... | collective-permute-start | bytes 1179656 | tf_op jit(solution)/shard_map/ppermute | solution.py:18
  107.5 10.5 %copy-start.3 = (bf16[384,512]{1,0:T(8,128)(2,1)S(1)}, bf16[384,512]{1,0:T(8,128)(2,1)}, u32[]{:S(2)}) copy-start(bf16[384,512]{1,0:T(8,128)(2,1)} %inner.3) | copy-start | bytes 1179652
  107.5 10.4 %collective-permute-start.13 = (bf16[384,512]{1,0:T(8,128)(2,1)}, bf16[384,512]{1,0:T(8,128)(2,1)S(1)}, u32[]{:S(2)}, u32[]{:S(2)}) collective-permute-start(bf16[384,512]{1,0:T(8,128)(2,1)} %inner.3), channel_id=1, source_target_pairs={{0,2},{1,3},{2,0},{3,1},{4,6},{5,7},{6,4},{7,5},{8,10},{9,11},{10,... | collective-permute-start | bytes 1179656 | tf_op jit(solution)/shard_map/ppermute | solution.py:18
  109.2 9.7 %collective-permute-start.17 = (f32[4]{0:T(128)S(1)}, f32[4]{0:T(128)S(1)}, u32[]{:S(2)}, u32[]{:S(2)}) collective-permute-start(f32[4]{0:T(128)S(1)} %select_reduce_fusion), channel_id=1, source_target_pairs={{0,8},{4,12},{8,0},{12,4},{16,24},{20,28},{24,16},{28,20},{1,9},{5... | collective-permute-start | bytes 56 | tf_op jit(solution)/shard_map/ppermute | solution.py:18
  109.3 11.2 %collective-permute-start.18 = (f32[4]{0:T(128)S(1)}, f32[4]{0:T(128)S(1)}, u32[]{:S(2)}, u32[]{:S(2)}) collective-permute-start(f32[4]{0:T(128)S(1)} %select_reduce_fusion), channel_id=1, source_target_pairs={{0,16},{4,20},{8,24},{12,28},{16,0},{20,4},{24,8},{28,12},{1,17},{... | collective-permute-start | bytes 56 | tf_op jit(solution)/shard_map/ppermute | solution.py:18
  109.4 14.9 %copy-start.15 = (bf16[48,4096]{1,0:T(8,128)(2,1)}, bf16[48,4096]{1,0:T(8,128)(2,1)S(1)}, u32[]{:S(2)}) copy-start(bf16[48,4096]{1,0:T(8,128)(2,1)S(1)} %collective-permute-done.15.refs_2_) | copy-start | bytes 1179652
  109.4 11.0 %collective-permute-start.19 = (f32[4]{0:T(128)S(1)}, f32[4]{0:T(128)S(1)}, u32[]{:S(2)}, u32[]{:S(2)}) collective-permute-start(f32[4]{0:T(128)S(1)} %select_reduce_fusion), channel_id=1, source_target_pairs={{0,24},{4,28},{8,16},{12,20},{16,8},{20,12},{24,0},{28,4},{1,25},{... | collective-permute-start | bytes 56 | tf_op jit(solution)/shard_map/ppermute | solution.py:18
  118.2 2.7 %collective-permute-start.16 = (bf16[384,1024]{1,0:T(8,128)(2,1)S(1)}, bf16[384,1024]{1,0:T(8,128)(2,1)S(1)}, u32[]{:S(2)}, u32[]{:S(2)}) collective-permute-start(bf16[384,1024]{1,0:T(8,128)(2,1)S(1)} %pad_maximum_fusion.2), channel_id=1, source_target_pairs={{0,1},{1,0},{2,3},{3,2},{4,5},{5,4},{6,7},{7,6},{8,9},{9,8},{10,11... | collective-permute-start | bytes 2359304 | tf_op jit(solution)/shard_map/ppermute | solution.py:18
  118.9 9.1 %collective-permute-start.2 = (bf16[4,144,256]{2,1,0:T(8,128)(2,1)S(1)}, bf16[4,144,256]{2,1,0:T(8,128)(2,1)}, u32[]{:S(2)}, u32[]{:S(2)}) collective-permute-start(bf16[4,144,256]{2,1,0:T(8,128)(2,1)S(1)} %copy-done.24), channel_id=1, source_target_pairs={{0,8},{4,12},{8,0},{12,4},{16,24},{20,28},{24,16},{28,20},{1,9},{5... | collective-permute-start | bytes 884744 | tf_op jit(solution)/shard_map/ppermute | solution.py:18
  118.9 12.2 %collective-permute-start.22 = (bf16[48,4096]{1,0:T(8,128)(2,1)S(1)}, bf16[48,4096]{1,0:T(8,128)(2,1)}, u32[]{:S(2)}, u32[]{:S(2)}) collective-permute-start(bf16[48,4096]{1,0:T(8,128)(2,1)S(1)} %get-tuple-element.214.refs_0_), channel_id=1, source_target_pairs={{0,2},{1,3},{2,0},{3,1},{4,6},{5,7},{6,4},{7,5},{8,10},{9,11},{10,... | collective-permute-start | bytes 1179656 | tf_op jit(solution)/shard_map/ppermute | solution.py:18
  122.8 23.5 %collective-permute-start.21 = (bf16[384,1024]{1,0:T(8,128)(2,1)}, bf16[384,1024]{1,0:T(8,128)(2,1)S(1)}, u32[]{:S(2)}, u32[]{:S(2)}) collective-permute-start(bf16[384,1024]{1,0:T(8,128)(2,1)} %convolution_convert_fusion.1), channel_id=1, source_target_pairs={{0,4},{4,0},{8,12},{12,8},{16,20},{20,16},{24,28},{28,24},{1,5},{5... | collective-permute-start | bytes 2359304 | tf_op jit(solution)/shard_map/ppermute | solution.py:18
  124.3 14.2 %collective-permute-start.23 = (bf16[48,4096]{1,0:T(8,128)(2,1)S(1)}, bf16[48,4096]{1,0:T(8,128)(2,1)}, u32[]{:S(2)}, u32[]{:S(2)}) collective-permute-start(bf16[48,4096]{1,0:T(8,128)(2,1)S(1)} %collective-permute-done.15.refs_2_), channel_id=1, source_target_pairs={{0,2},{1,3},{2,0},{3,1},{4,6},{5,7},{6,4},{7,5},{8,10},{9,11},{10,... | collective-permute-start | bytes 1179656 | tf_op jit(solution)/shard_map/ppermute | solution.py:18
  125.5 36.5 %collective-permute-start.26 = (bf16[96,4096]{1,0:T(8,128)(2,1)}, bf16[96,4096]{1,0:T(8,128)(2,1)S(1)}, u32[]{:S(2)}, u32[]{:S(2)}) collective-permute-start(bf16[96,4096]{1,0:T(8,128)(2,1)} %bitcast.14), channel_id=1, source_target_pairs={{0,4},{4,0},{8,12},{12,8},{16,20},{20,16},{24,28},{28,24},{1,5},{5... | collective-permute-start | bytes 2359304 | tf_op jit(solution)/shard_map/ppermute | solution.py:18
  138.5 15.6 %collective-permute-start.20 = (bf16[4,144,256]{2,1,0:T(8,128)(2,1)}, bf16[4,144,256]{2,1,0:T(8,128)(2,1)}, u32[]{:S(2)}, u32[]{:S(2)}) collective-permute-start(bf16[4,144,256]{2,1,0:T(8,128)(2,1)} %get-tuple-element.209), channel_id=1, source_target_pairs={{0,16},{4,20},{8,24},{12,28},{16,0},{20,4},{24,8},{28,12},{1,17},{... | collective-permute-start | bytes 884744 | tf_op jit(solution)/shard_map/ppermute | solution.py:18
  144.8 16.5 %collective-permute-start.24 = (bf16[192,512]{1,0:T(8,128)(2,1)}, bf16[192,512]{1,0:T(8,128)(2,1)S(1)}, u32[]{:S(2)}, u32[]{:S(2)}) collective-permute-start(bf16[192,512]{1,0:T(8,128)(2,1)} %inner.4), channel_id=1, source_target_pairs={{0,2},{1,3},{2,0},{3,1},{4,6},{5,7},{6,4},{7,5},{8,10},{9,11},{10,... | collective-permute-start | bytes 589832 | tf_op jit(solution)/shard_map/ppermute | solution.py:18
  161.4 9.4 %collective-permute-start.25 = (bf16[192,1024]{1,0:T(8,128)(2,1)S(1)}, bf16[192,1024]{1,0:T(8,128)(2,1)S(1)}, u32[]{:S(2)}, u32[]{:S(2)}) collective-permute-start(bf16[192,1024]{1,0:T(8,128)(2,1)S(1)} %pad_maximum_fusion.5), channel_id=1, source_target_pairs={{0,1},{1,0},{2,3},{3,2},{4,5},{5,4},{6,7},{7,6},{8,9},{9,8},{10,11... | collective-permute-start | bytes 1179656 | tf_op jit(solution)/shard_map/ppermute | solution.py:18
  169.2 20.8 %collective-permute-start.28 = (bf16[192,512]{1,0:T(8,128)(2,1)}, bf16[192,512]{1,0:T(8,128)(2,1)S(1)}, u32[]{:S(2)}, u32[]{:S(2)}) collective-permute-start(bf16[192,512]{1,0:T(8,128)(2,1)} %inner.5), channel_id=1, source_target_pairs={{0,2},{1,3},{2,0},{3,1},{4,6},{5,7},{6,4},{7,5},{8,10},{9,11},{10,... | collective-permute-start | bytes 589832 | tf_op jit(solution)/shard_map/ppermute | solution.py:18
  176.9 13.1 %copy-start.11 = (bf16[192,512]{1,0:T(8,128)(2,1)S(1)}, bf16[192,512]{1,0:T(8,128)(2,1)}, u32[]{:S(2)}) copy-start(bf16[192,512]{1,0:T(8,128)(2,1)} %inner.5) | copy-start | bytes 589828
  187.2 15.7 %collective-permute-start.27 = (bf16[256,4096]{1,0:T(8,128)(2,1)}, bf16[256,4096]{1,0:T(8,128)(2,1)S(1)}, u32[]{:S(2)}, u32[]{:S(2)}) collective-permute-start(bf16[256,4096]{1,0:T(8,128)(2,1)} %get-tuple-element.256), channel_id=1, source_target_pairs={{0,1},{1,0},{2,3},{3,2},{4,5},{5,4},{6,7},{7,6},{8,9},{9,8},{10,11... | collective-permute-start | bytes 6291464 | tf_op jit(solution)/shard_map/ppermute | solution.py:18
  187.4 12.4 %copy-start.19 = (bf16[192,1024]{1,0:T(8,128)(2,1)S(1)}, bf16[192,1024]{1,0:T(8,128)(2,1)}, u32[]{:S(2)}) copy-start(bf16[192,1024]{1,0:T(8,128)(2,1)} %convolution_convert_fusion.4) | copy-start | bytes 1179652
  187.4 26.9 %collective-permute-start.32 = (bf16[256,1024]{1,0:T(8,128)(2,1)S(1)}, bf16[256,1024]{1,0:T(8,128)(2,1)S(1)}, u32[]{:S(2)}, u32[]{:S(2)}) collective-permute-start(bf16[256,1024]{1,0:T(8,128)(2,1)S(1)} %bitcast.106), channel_id=1, source_target_pairs={{0,24},{4,28},{8,16},{12,20},{16,8},{20,12},{24,0},{28,4},{1,25},{... | collective-permute-start | bytes 1572872 | tf_op jit(solution)/shard_map/ppermute | solution.py:18
  188.5 11.2 %collective-permute-start.30 = (bf16[192,1024]{1,0:T(8,128)(2,1)}, bf16[192,1024]{1,0:T(8,128)(2,1)S(1)}, u32[]{:S(2)}, u32[]{:S(2)}) collective-permute-start(bf16[192,1024]{1,0:T(8,128)(2,1)} %convolution_convert_fusion.5), channel_id=1, source_target_pairs={{0,4},{4,0},{8,12},{12,8},{16,20},{20,16},{24,28},{28,24},{1,5},{5... | collective-permute-start | bytes 1179656 | tf_op jit(solution)/shard_map/ppermute | solution.py:18
  190.1 10.0 %copy-start.10 = (bf16[1024,1024]{1,0:T(8,128)(2,1)S(1)}, bf16[1024,1024]{1,0:T(8,128)(2,1)}, u32[]{:S(2)}) copy-start(bf16[1024,1024]{1,0:T(8,128)(2,1)} %pad_maximum_fusion) | copy-start | bytes 6291460
  190.2 9.9 %collective-permute-start.29 = (bf16[192,1024]{1,0:T(8,128)(2,1)S(1)}, bf16[192,1024]{1,0:T(8,128)(2,1)S(1)}, u32[]{:S(2)}, u32[]{:S(2)}) collective-permute-start(bf16[192,1024]{1,0:T(8,128)(2,1)S(1)} %pad_maximum_fusion.7), channel_id=1, source_target_pairs={{0,1},{1,0},{2,3},{3,2},{4,5},{5,4},{6,7},{7,6},{8,9},{9,8},{10,11... | collective-permute-start | bytes 1179656 | tf_op jit(solution)/shard_map/ppermute | solution.py:18
  200.0 36.4 %collective-permute-start.35 = (bf16[256,1024]{1,0:T(8,128)(2,1)S(1)}, bf16[256,1024]{1,0:T(8,128)(2,1)S(1)}, u32[]{:S(2)}, u32[]{:S(2)}) collective-permute-start(bf16[256,1024]{1,0:T(8,128)(2,1)S(1)} %bitcast.104), channel_id=1, source_target_pairs={{0,16},{4,20},{8,24},{12,28},{16,0},{20,4},{24,8},{28,12},{1,17},{... | collective-permute-start | bytes 1572872 | tf_op jit(solution)/shard_map/ppermute | solution.py:18
  200.7 10.2 %collective-permute-start.33 = (bf16[192,1024]{1,0:T(8,128)(2,1)S(1)}, bf16[192,1024]{1,0:T(8,128)(2,1)S(1)}, u32[]{:S(2)}, u32[]{:S(2)}) collective-permute-start(bf16[192,1024]{1,0:T(8,128)(2,1)S(1)} %convolution_convert_fusion.3), channel_id=1, source_target_pairs={{0,4},{4,0},{8,12},{12,8},{16,20},{20,16},{24,28},{28,24},{1,5},{5... | collective-permute-start | bytes 1179656 | tf_op jit(solution)/shard_map/ppermute | solution.py:18
  203.0 11.4 %copy-start.20 = (s32[2,512]{1,0:T(2,128)S(1)}, s32[2,512]{1,0:T(2,128)}, u32[]{:S(2)}) copy-start(s32[2,512]{1,0:T(2,128)} %multiply_add_fusion.slot_ref) | copy-start | bytes 12292
  203.0 11.4 %copy-start.21 = (f32[512,2]{0,1:T(2,128)S(1)}, f32[512,2]{0,1:T(2,128)}, u32[]{:S(2)}) copy-start(f32[512,2]{0,1:T(2,128)} %param.24) | copy-start | bytes 12292
  203.3 11.7 %copy-start.23 = (s32[256]{0:T(256)S(1)}, s32[256]{0:T(256)}, u32[]{:S(2)}) copy-start(s32[256]{0:T(256)} %iota_add_fusion.3) | copy-start | bytes 3076
  203.3 24.0 %collective-permute-start.31 = (bf16[128,4096]{1,0:T(8,128)(2,1)S(1)}, bf16[128,4096]{1,0:T(8,128)(2,1)S(1)}, u32[]{:S(2)}, u32[]{:S(2)}) collective-permute-start(bf16[128,4096]{1,0:T(8,128)(2,1)S(1)} %add_convert_fusion.2), channel_id=1, source_target_pairs={{0,2},{1,3},{2,0},{3,1},{4,6},{5,7},{6,4},{7,5},{8,10},{9,11},{10,... | collective-permute-start | bytes 3145736 | tf_op jit(solution)/shard_map/ppermute | solution.py:18
  211.2 24.5 %collective-permute-start.34 = (bf16[256,1024]{1,0:T(8,128)(2,1)S(1)}, bf16[256,1024]{1,0:T(8,128)(2,1)S(1)}, u32[]{:S(2)}, u32[]{:S(2)}) collective-permute-start(bf16[256,1024]{1,0:T(8,128)(2,1)S(1)} %bitcast.105), channel_id=1, source_target_pairs={{0,8},{4,12},{8,0},{12,4},{16,24},{20,28},{24,16},{28,20},{1,9},{5... | collective-permute-start | bytes 1572872 | tf_op jit(solution)/shard_map/ppermute | solution.py:18
  215.0 12.3 %copy-start.7 = (bf16[256,4096]{1,0:T(8,128)(2,1)S(1)}, bf16[256,4096]{1,0:T(8,128)(2,1)}, u32[]{:S(2)}) copy-start(bf16[256,4096]{1,0:T(8,128)(2,1)} %copy-done.6) | copy-start | bytes 6291460
  (14 other events, 46.2 us)
